TPU v7x, 512 devices: a whole 4x8x8 slice. The times are simulated.
512 devices in a mesh: kv: 64 (over z, y), tp: 8 (over x, core).
Axes of the slice: x: 4, y: 8, z: 8, core: 2. Of those that a mesh axis runs over, the one named last changes fastest.
Arguments:
- hidden_in: bfloat16 [256, 2048], P('tp', 'kv'), may hold values from -20 to 20
- gain_before: float32 [2048], P('kv'), may hold values from 0.1 to 1.9
- gate_before: bfloat16 [2048, 5632], P('kv', 'tp'), may hold values from -0.125 to 0.125
- lift_before: bfloat16 [2048, 5632], P('kv', 'tp'), may hold values from -0.125 to 0.125
- drop_before: bfloat16 [5632, 2048], P('tp', 'kv'), may hold values from -0.078125 to 0.078125
- mixer_gain: float32 [2048], P('kv'), may hold values from 0.1 to 1.9
- value_proj: bfloat16 [2048, 2048], P('kv', 'tp'), may hold values from -0.125 to 0.125
- gate_proj: bfloat16 [2048, 2048], P('kv', 'tp'), may hold values from -0.125 to 0.125
- key_proj: bfloat16 [2048, 1024], P('kv', 'tp'), may hold values from -0.125 to 0.125
- query_proj: bfloat16 [2048, 1024], P('kv', 'tp'), may hold values from -0.125 to 0.125
- step_proj: bfloat16 [2048, 32], P('kv'), may hold values from -0.125 to 0.125
- value_taps: float32 [4, 2048], P(None, 'tp'), may hold values from -3 to 3
- key_taps: float32 [4, 1024], P(None, 'tp'), may hold values from -3 to 3
- query_taps: float32 [4, 1024], P(None, 'tp'), may hold values from -3 to 3
- value_past: bfloat16 [256, 3, 2048], P('kv', None, 'tp'), may hold values from -6 to 6
- key_past: bfloat16 [256, 3, 1024], P('kv', None, 'tp'), may hold values from -6 to 6
- query_past: bfloat16 [256, 3, 1024], P('kv', None, 'tp'), may hold values from -6 to 6
- decay_rate: float32 [32], P('tp'), may hold values from 0.05 to 1
- block_state: float32 [256, 32, 64, 128], P('kv', 'tp'), may hold values from -24 to 24
- block_keys: bfloat16 [256, 128, 1024], P('kv', None, 'tp'), may hold values from -6 to 6
- block_values: bfloat16 [256, 128, 2048], P('kv', None, 'tp'), may hold values from -6 to 6
- block_steps: float32 [256, 128, 32], P('kv', None, 'tp'), may hold values from 0.2 to 2
- block_decay: float32 [256, 128, 32], P('kv', None, 'tp'), may hold values from -1.25 to 0
- lengths: int32 [256], P('kv'), may hold values from 1 to 128, 8192 in all
- head_gain: float32 [2048], P('tp'), may hold values from 0.1 to 1.9
- out_proj: bfloat16 [2048, 2048], P('tp', 'kv'), may hold values from -0.125 to 0.125
- gain_after: float32 [2048], P('kv'), may hold values from 0.1 to 1.9
- gate_after: bfloat16 [2048, 5632], P('kv', 'tp'), may hold values from -0.125 to 0.125
- lift_after: bfloat16 [2048, 5632], P('kv', 'tp'), may hold values from -0.125 to 0.125
- drop_after: bfloat16 [5632, 2048], P('tp', 'kv'), may hold values from -0.078125 to 0.078125
Outputs:
- hidden_out: bfloat16 [256, 2048], P('tp', 'kv')
Inputs may be any that keep to these rules, and one draw needn't show every extreme that they name: `lengths`: some sequence has all 128 positions filled.
All inputs are finite; a program needn't handle non-finite values. No bound on the sum of `lengths` on one device may be relied on, other than what follows from the above.
Results may differ from a plain program's by a relative error of at most 0.014.
Values may be sent and summed in bfloat16 or wider, within the bound.
A program may use at most 64 MiB of HBM per device.

v0:
```python
import math

import jax
import jax.numpy as jnp
from jax import lax
from jax.sharding import Mesh
from jax.sharding import PartitionSpec as P

D = 2048
GROUPS = 8
HEADS = 32
KV = ("kv_0", "kv_1")


EPSILON = 1e-06


def copy_for_each(shard, axis):
    size = lax.axis_size(axis)
    return lax.all_to_all(
        jnp.broadcast_to(shard[None], (size, *shard.shape)), axis, 0, 0, tiled=True
    )


def joined_along(pieces, dim):
    shape = list(pieces.shape[1:])
    shape[dim] *= pieces.shape[0]
    return jnp.moveaxis(pieces, 0, dim).reshape(shape)


def collect(shard, axis, dim):
    pieces = copy_for_each(shard, axis)
    return joined_along(pieces, dim)


def cut_along(shard, dim, size):
    shape = shard.shape
    pieces = shard.reshape(*shape[:dim], size, shape[dim] // size, *shape[dim + 1 :])
    return jnp.moveaxis(pieces, dim, 0)


def sum_at_owner(shard, axis, dim):
    size = lax.axis_size(axis)
    pieces = lax.all_to_all(cut_along(shard, dim, size), axis, 0, 0, tiled=True)
    return jnp.sum(pieces.astype(jnp.float32), axis=0)


def by_axis(shard, axes):
    for axis in axes:
        shard = lax.psum(shard, axis)
    return shard


def side_by_side(arrays, axis, dim, along):
    both = jnp.concatenate(arrays, axis=along)
    out, at, done = (sum_at_owner(both, axis, dim), 0, [])
    for a in arrays:
        done.append(lax.slice_in_dim(out, at, at + a.shape[along], axis=along))
        at += a.shape[along]
    return tuple(done)


def in_one_piece(arrays, axis, dim, along):
    widths = [math.prod(a.shape[along:]) for a in arrays]
    both = jnp.concatenate(
        [a.reshape(*a.shape[:along], w) for a, w in zip(arrays, widths)], axis=along
    )
    out = sum_at_owner(both, axis, dim)
    pieces = jnp.split(out, [sum(widths[:k]) for k in range(1, len(widths))], axis=along)
    return tuple((b.reshape(*out.shape[:along], *a.shape[along:]) for a, b in zip(arrays, pieces)))


def gather_rows(rows_in, gain_vec):
    whole_rows = collect(rows_in, "tp", 0)
    values = whole_rows.astype(jnp.float32)
    squares = jnp.sum(values * values, axis=1)
    scaled = (values * gain_vec[None, :]).astype(jnp.bfloat16)
    return (scaled, squares)


def inverse_scale(totals):
    return lax.rsqrt(totals / D + EPSILON)[:, None]


def own_rows(totals, row_count):
    return lax.dynamic_slice_in_dim(totals, lax.axis_index(KV) * row_count, row_count, 0)


def finish(partial_value):
    return sum_at_owner(partial_value.astype(jnp.float32).astype(jnp.bfloat16), "tp", 0)


def half_mlp(rows_in, gain_vec, gate_weight, lift_weight, drop_weight, row_count):
    scaled, squares = gather_rows(rows_in, gain_vec)
    totals = by_axis(squares, KV)
    gate_part = jnp.dot(scaled, gate_weight, preferred_element_type=jnp.float32)
    lift_part = jnp.dot(scaled, lift_weight, preferred_element_type=jnp.float32)
    gate_sum, lift_sum = side_by_side(
        (gate_part.astype(jnp.bfloat16), lift_part.astype(jnp.bfloat16)), KV, 0, 1
    )
    row_scale = inverse_scale(own_rows(totals, row_count))
    hidden = (jax.nn.silu(gate_sum * row_scale) * (lift_sum * row_scale)).astype(jnp.bfloat16)
    partial_value = jnp.dot(
        collect(hidden, KV, 0), drop_weight, preferred_element_type=jnp.float32
    ).astype(jnp.bfloat16)
    return finish(partial_value)


def convolve(past_rows, taps, newest):
    earlier = jnp.sum(past_rows.astype(jnp.float32) * taps[None, :-1, :], axis=1)
    return jax.nn.silu(earlier + taps[-1][None, :] * newest)


def mixer(
    rows_in,
    mixer_gain,
    value_proj,
    gate_proj,
    key_proj,
    query_proj,
    step_proj,
    value_taps,
    key_taps,
    query_taps,
    value_past,
    key_past,
    query_past,
    decay_rate,
    block_state,
    block_keys,
    block_values,
    block_steps,
    block_decay,
    lengths,
    head_gain,
    out_proj,
):
    scaled, squares = gather_rows(rows_in, mixer_gain)
    seq_count = lengths.shape[0]
    value_part = jnp.dot(scaled, value_proj, preferred_element_type=jnp.float32)
    gate_part = jnp.dot(scaled, gate_proj, preferred_element_type=jnp.float32)
    key_part = jnp.dot(scaled, key_proj, preferred_element_type=jnp.float32)
    query_part = jnp.dot(scaled, query_proj, preferred_element_type=jnp.float32)
    step_part = jnp.dot(scaled, step_proj, preferred_element_type=jnp.float32)
    value_raw, gate_raw, key_raw, query_raw, step_all, totals = in_one_piece(
        (
            value_part.astype(jnp.bfloat16),
            gate_part.astype(jnp.bfloat16),
            key_part.astype(jnp.bfloat16),
            query_part.astype(jnp.bfloat16),
            step_part.astype(jnp.bfloat16),
            squares.astype(jnp.bfloat16),
        ),
        KV,
        0,
        1,
    )
    row_scale = inverse_scale(totals)
    heads_here = decay_rate.shape[0]
    step_raw = (
        lax.dynamic_slice_in_dim(step_all, lax.axis_index("tp") * heads_here, heads_here, 1)
        * row_scale
    )
    new_value = convolve(value_past, value_taps, value_raw * row_scale)
    gate_vals = gate_raw * row_scale
    new_key = convolve(key_past, key_taps, key_raw * row_scale)
    new_query = convolve(query_past, query_taps, query_raw * row_scale)
    step_size = jax.nn.softplus(step_raw)
    new_decay = -decay_rate[None, :] * step_size
    block_len = block_keys.shape[1]
    head_dim = block_state.shape[2]
    state_size = block_state.shape[3]
    per_group = HEADS // GROUPS
    group_count = heads_here // per_group
    live_mask = (jnp.arange(block_len, dtype=jnp.int32)[None, :] < (lengths - 1)[:, None])[
        :, :, None
    ]
    masked = jnp.where(live_mask, block_decay, 0.0)
    running = jnp.cumsum(masked, axis=1)
    block_total = running[:, -1, :]
    tail_sum = block_total[:, None, :] - running
    query_round = new_query.astype(jnp.bfloat16).reshape(seq_count, group_count, state_size)
    scores = jnp.einsum(
        "slgn,sgn->slg",
        block_keys.reshape(seq_count, block_len, group_count, state_size),
        query_round,
        preferred_element_type=jnp.float32,
    )
    scores = jnp.repeat(scores, per_group, axis=2)
    weights = jnp.where(
        live_mask, jnp.exp(tail_sum + new_decay[:, None, :]) * block_steps * scores, 0.0
    ).astype(jnp.bfloat16)
    from_block = jnp.einsum(
        "slh,slhp->shp",
        weights,
        block_values.reshape(seq_count, block_len, heads_here, head_dim),
        preferred_element_type=jnp.float32,
    )
    query_heads = jnp.repeat(
        new_query.reshape(seq_count, group_count, state_size), per_group, axis=1
    )
    source_state = jnp.einsum(
        "shpn,shn->shp", block_state, query_heads, precision=lax.Precision.HIGHEST
    )
    source_state = source_state * jnp.exp(block_total + new_decay)[:, :, None]
    self_score = jnp.repeat(
        jnp.sum((new_query * new_key).reshape(seq_count, group_count, state_size), axis=2),
        per_group,
        axis=1,
    )
    from_token = (step_size * self_score)[:, :, None] * new_value.reshape(
        seq_count, heads_here, head_dim
    )
    gated_out = (source_state + from_block + from_token) * jax.nn.silu(
        gate_vals.reshape(seq_count, heads_here, head_dim)
    )
    normed = gated_out * lax.rsqrt(jnp.mean(gated_out * gated_out, axis=2, keepdims=True) + EPSILON)
    normed = normed * head_gain.reshape(heads_here, head_dim)[None]
    mixed_rows = normed.reshape(seq_count, heads_here * head_dim).astype(jnp.bfloat16)
    partial_value = jnp.dot(
        collect(mixed_rows, KV, 0), out_proj, preferred_element_type=jnp.float32
    ).astype(jnp.bfloat16)
    return finish(partial_value)


def on_device(
    hidden_in,
    gain_before,
    gate_before,
    lift_before,
    drop_before,
    mixer_gain,
    value_proj,
    gate_proj,
    key_proj,
    query_proj,
    step_proj,
    value_taps,
    key_taps,
    query_taps,
    value_past,
    key_past,
    query_past,
    decay_rate,
    block_state,
    block_keys,
    block_values,
    block_steps,
    block_decay,
    lengths,
    head_gain,
    out_proj,
    gain_after,
    gate_after,
    lift_after,
    drop_after,
):
    seq_count = lengths.shape[0]
    section_one = (
        hidden_in.astype(jnp.float32)
        + 0.5 * half_mlp(hidden_in, gain_before, gate_before, lift_before, drop_before, seq_count)
    ).astype(jnp.bfloat16)
    branch_mix = mixer(
        section_one,
        mixer_gain,
        value_proj,
        gate_proj,
        key_proj,
        query_proj,
        step_proj,
        value_taps,
        key_taps,
        query_taps,
        value_past,
        key_past,
        query_past,
        decay_rate,
        block_state,
        block_keys,
        block_values,
        block_steps,
        block_decay,
        lengths,
        head_gain,
        out_proj,
    )
    section_two = (section_one.astype(jnp.float32) + branch_mix).astype(jnp.bfloat16)
    return (
        section_two.astype(jnp.float32)
        + 0.5 * half_mlp(section_two, gain_after, gate_after, lift_after, drop_after, seq_count)
    ).astype(jnp.bfloat16)


def solution(mesh):
    finer = Mesh(mesh.devices.reshape(8, 8, mesh.shape["tp"]), ("kv_0", "kv_1", "tp"))
    return jax.shard_map(
        on_device,
        mesh=finer,
        in_specs=(
            P("tp", KV),
            P(KV),
            P(KV, "tp"),
            P(KV, "tp"),
            P("tp", KV),
            P(KV),
            P(KV, "tp"),
            P(KV, "tp"),
            P(KV, "tp"),
            P(KV, "tp"),
            P(KV, None),
            P(None, "tp"),
            P(None, "tp"),
            P(None, "tp"),
            P(KV, None, "tp"),
            P(KV, None, "tp"),
            P(KV, None, "tp"),
            P("tp"),
            P(KV, "tp", None, None),
            P(KV, None, "tp"),
            P(KV, None, "tp"),
            P(KV, None, "tp"),
            P(KV, None, "tp"),
            P(KV),
            P("tp"),
            P("tp", KV),
            P(KV),
            P(KV, "tp"),
            P(KV, "tp"),
            P("tp", KV),
        ),
        out_specs=P("tp", KV),
        check_vma=False,
    )
```

profile of v0, /device:TPU:1, one launch (start us, length us, event | category | flops | bytes accessed | tf_op | source)
XLA Modules:
  0.0 266.2 jit_solution(3855109655083443415)
XLA Ops:
  0.0 0.8 broadcast_in_dim.24
  0.8 0.1 reshape.172
  0.9 13.8 %all_to_all.60 = bf16[8,2,512]{2,1,0:T(2,128)(2,1)S(1)} all-to-all(bf16[8,2,512]{2,1,0:T(2,128)(2,1)S(1)} %reshape.172), channel_id=1, replica_groups=mesh['kv_0'=8,'kv_1'=8,'tp'=8] {'tp'}, dimensions={0} | all-to-all | bytes 32768 | tf_op jit(solution)/shard_map/all_to_all | solution.py:20
  14.8 0.7 fusion.2
  15.5 1.1 convolution_convert_fusion.2
  16.6 0.3 convolution_convert_fusion.3
  17.0 0.3 copy.104
  17.3 1.0 reshape.144
  18.4 12.7 %all-to-all-start.1 = ((bf16[64,4,1408]{2,1,0:T(4,128)(2,1)}), bf16[64,4,1408]{2,1,0:T(4,128)(2,1)S(1)}, u32[]{:S(2)}, u32[]{:S(2)}) async-start(bf16[64,4,1408]{2,1,0:T(4,128)(2,1)} %reshape.144), calls=%async_computation.1 | async-start | bytes 1441792 | tf_op jit(solution)/shard_map/all_to_all | solution.py:44
  31.3 18.3 %psum.28 = f32[256]{0:T(256)S(1)} all-reduce(f32[256]{0:T(256)S(1)} %reduce_sum.132), channel_id=1, replica_groups=mesh['kv_0'=8,'kv_1'=8,'tp'=8] {'kv_0'}, use_global_device_ids=true, to_apply=%region_2.0 | all-reduce | flops 256 | bytes 2048 | tf_op jit(solution)/shard_map/psum | solution.py:50
  49.6 17.1 %psum.29 = f32[256]{0:T(256)S(1)} all-reduce(f32[256]{0:T(256)S(1)} %psum.28), channel_id=1, replica_groups=mesh['kv_0'=8,'kv_1'=8,'tp'=8] {'kv_1'}, use_global_device_ids=true, to_apply=%region_3.0 | all-reduce | flops 256 | bytes 2048 | tf_op jit(solution)/shard_map/psum | solution.py:50
  66.8 0.3 convert_reduce_fusion.1
  67.3 22.5 %all_to_all.61 = bf16[64,4,704]{2,1,0:T(4,128)(2,1)S(1)} all-to-all(bf16[64,4,704]{2,1,0:T(4,128)(2,1)S(1)} %broadcast_in_dim.25), channel_id=1, replica_groups=mesh['kv_0'=8,'kv_1'=8,'tp'=8] {'kv_0','kv_1'}, dimensions={0} | all-to-all | bytes 720896 | tf_op jit(solution)/shard_map/all_to_all | solution.py:20
  89.8 0.2 reshape.145
  90.0 0.2 convolution_convert_fusion.11
  90.3 0.2 reshape.146
  90.5 0.7 reshape.174
  91.2 13.5 %all-to-all-start.3 = ((bf16[8,2,512]{2,1,0:T(2,128)(2,1)}), bf16[8,2,512]{2,1,0:T(2,128)(2,1)S(1)}, u32[]{:S(2)}, u32[]{:S(2)}) async-start(bf16[8,2,512]{2,1,0:T(2,128)(2,1)} %reshape.174), calls=%async_computation.3 | async-start | bytes 32768 | tf_op jit(solution)/shard_map/all_to_all | solution.py:44
  104.8 4.6 %all-to-all-done.3 = bf16[8,2,512]{2,1,0:T(2,128)(2,1)S(1)} async-done(((bf16[8,2,512]{2,1,0:T(2,128)(2,1)}), bf16[8,2,512]{2,1,0:T(2,128)(2,1)S(1)}, u32[]{:S(2)}, u32[]{:S(2)}) %all-to-all-start.3) | async-done | bytes 16416 | tf_op jit(solution)/shard_map/all_to_all | solution.py:44
  109.6 0.7 reshape.176
  110.3 4.1 %all-to-all-start.4 = ((bf16[8,2,512]{2,1,0:T(2,128)(2,1)}), bf16[8,2,512]{2,1,0:T(2,128)(2,1)S(1)}, u32[]{:S(2)}, u32[]{:S(2)}) async-start(bf16[8,2,512]{2,1,0:T(2,128)(2,1)} %reshape.176), calls=%async_computation.4 | async-start | bytes 32768 | tf_op jit(solution)/shard_map/all_to_all | solution.py:20
  114.4 4.7 %all-to-all-done.4 = bf16[8,2,512]{2,1,0:T(2,128)(2,1)S(1)} async-done(((bf16[8,2,512]{2,1,0:T(2,128)(2,1)}), bf16[8,2,512]{2,1,0:T(2,128)(2,1)S(1)}, u32[]{:S(2)}, u32[]{:S(2)}) %all-to-all-start.4) | async-done | bytes 16416 | tf_op jit(solution)/shard_map/all_to_all | solution.py:20
  119.4 0.2 convolution_convert_fusion.5
  119.6 0.2 convolution_convert_fusion.4
  119.8 0.2 convolution_convert_fusion.9
  119.9 0.1 copy.108
  120.1 0.1 convolution_convert_fusion.7
  120.2 0.1 convolution_convert_fusion.6
  120.4 0.2 convert_element_type.209
  120.6 1.2 concatenate.26
  121.7 4.6 %all-to-all-start.5 = ((bf16[64,4,801]{2,1,0:T(4,128)(2,1)}), bf16[64,4,801]{2,1,0:T(4,128)(2,1)S(1)}, u32[]{:S(2)}, u32[]{:S(2)}) async-start(bf16[64,4,801]{2,1,0:T(4,128)(2,1)} %concatenate.26), calls=%async_computation.5 | async-start | bytes 917504 | tf_op jit(solution)/shard_map/all_to_all | solution.py:44
  126.5 0.1 copy.110
  126.7 0.3 reduce_window_sum.11
  127.1 0.2 copy-done.1
  127.3 0.2 copy.112
  127.7 15.2 %all-to-all-done.5 = bf16[64,4,801]{2,1,0:T(4,128)(2,1)S(1)} async-done(((bf16[64,4,801]{2,1,0:T(4,128)(2,1)}), bf16[64,4,801]{2,1,0:T(4,128)(2,1)S(1)}, u32[]{:S(2)}, u32[]{:S(2)}) %all-to-all-start.5) | async-done | bytes 410144 | tf_op jit(solution)/shard_map/all_to_all | solution.py:44
  142.9 0.2 convert_reduce_fusion.2
  143.1 0.2 fusion.18
  143.3 0.2 fusion.23
  143.7 0.2 fusion.21
  144.1 0.2 fusion.8
  144.4 0.9 fusion.25
  145.3 0.2 multiply_reduce_fusion.4
  145.7 17.5 %all_to_all.62 = bf16[64,4,256]{2,1,0:T(4,128)(2,1)S(1)} all-to-all(bf16[64,4,256]{2,1,0:T(4,128)(2,1)S(1)} %broadcast_in_dim.33), channel_id=1, replica_groups=mesh['kv_0'=8,'kv_1'=8,'tp'=8] {'kv_0','kv_1'}, dimensions={0} | all-to-all | bytes 262144 | tf_op jit(solution)/shard_map/all_to_all | solution.py:20
  163.3 0.1 convolution_convert_fusion.8
  163.5 0.1 reshape.154
  163.6 0.1 reshape.178
  163.8 9.8 %all_to_all.63 = bf16[8,2,512]{2,1,0:T(2,128)(2,1)S(1)} all-to-all(bf16[8,2,512]{2,1,0:T(2,128)(2,1)S(1)} %reshape.178), channel_id=1, replica_groups=mesh['kv_0'=8,'kv_1'=8,'tp'=8] {'tp'}, dimensions={0} | all-to-all | bytes 32768 | tf_op jit(solution)/shard_map/all_to_all | solution.py:44
  173.8 0.1 reshape.180
  173.9 7.7 %all_to_all.64 = bf16[8,2,512]{2,1,0:T(2,128)(2,1)S(1)} all-to-all(bf16[8,2,512]{2,1,0:T(2,128)(2,1)S(1)} %reshape.180), channel_id=1, replica_groups=mesh['kv_0'=8,'kv_1'=8,'tp'=8] {'tp'}, dimensions={0} | all-to-all | bytes 32768 | tf_op jit(solution)/shard_map/all_to_all | solution.py:20
  181.7 0.3 convolution_convert_fusion
  182.1 0.3 convolution_convert_fusion.1
  182.4 0.3 copy.116
  182.8 1.0 reshape.155
  183.8 4.8 %all-to-all-start.9 = ((bf16[64,4,1408]{2,1,0:T(4,128)(2,1)}), bf16[64,4,1408]{2,1,0:T(4,128)(2,1)S(1)}, u32[]{:S(2)}, u32[]{:S(2)}) async-start(bf16[64,4,1408]{2,1,0:T(4,128)(2,1)} %reshape.155), calls=%async_computation.9 | async-start | bytes 1441792 | tf_op jit(solution)/shard_map/all_to_all | solution.py:44
  188.8 16.0 %psum.30 = f32[256]{0:T(256)S(1)} all-reduce(f32[256]{0:T(256)S(1)} %reduce_sum.144), channel_id=1, replica_groups=mesh['kv_0'=8,'kv_1'=8,'tp'=8] {'kv_0'}, use_global_device_ids=true, to_apply=%region_16.17 | all-reduce | flops 256 | bytes 2048 | tf_op jit(solution)/shard_map/psum | solution.py:50
  204.8 18.2 %psum.31 = f32[256]{0:T(256)S(1)} all-reduce(f32[256]{0:T(256)S(1)} %psum.30), channel_id=1, replica_groups=mesh['kv_0'=8,'kv_1'=8,'tp'=8] {'kv_1'}, use_global_device_ids=true, to_apply=%region_17.18 | all-reduce | flops 256 | bytes 2048 | tf_op jit(solution)/shard_map/psum | solution.py:50
  223.1 0.3 convert_reduce_fusion
  223.6 23.7 %all_to_all.65 = bf16[64,4,704]{2,1,0:T(4,128)(2,1)S(1)} all-to-all(bf16[64,4,704]{2,1,0:T(4,128)(2,1)S(1)} %broadcast_in_dim.35), channel_id=1, replica_groups=mesh['kv_0'=8,'kv_1'=8,'tp'=8] {'kv_0','kv_1'}, dimensions={0} | all-to-all | bytes 720896 | tf_op jit(solution)/shard_map/all_to_all | solution.py:20
  247.3 0.2 reshape.156
  247.5 0.2 convolution_convert_fusion.10
  247.7 0.2 reshape.157
  248.0 17.4 %all_to_all.66 = bf16[8,2,512]{2,1,0:T(2,128)(2,1)S(1)} all-to-all(bf16[8,2,512]{2,1,0:T(2,128)(2,1)S(1)} %reshape.182), channel_id=1, replica_groups=mesh['kv_0'=8,'kv_1'=8,'tp'=8] {'tp'}, dimensions={0} | all-to-all | bytes 32768 | tf_op jit(solution)/shard_map/all_to_all | solution.py:44
  265.5 0.7 copy.119
  (119 shorter events, 3.5 us)
Async XLA Ops:
  0.0 144.4 %copy-start = (f32[4,4,64,128]{3,2,1,0:T(8,128)S(1)}, f32[4,4,64,128]{3,2,1,0:T(8,128)}, u32[]{:S(2)}) copy-start(f32[4,4,64,128]{3,2,1,0:T(8,128)} %param.48) | copy-start | bytes 1572868
  0.0 16.6 %copy-start.3 = (bf16[32,704]{1,0:T(8,128)(2,1)S(1)}, bf16[32,704]{1,0:T(8,128)(2,1)}, u32[]{:S(2)}) copy-start(bf16[32,704]{1,0:T(8,128)(2,1)} %param.32) | copy-start | bytes 135172
  18.4 48.4 %all-to-all-start.1 = ((bf16[64,4,1408]{2,1,0:T(4,128)(2,1)}), bf16[64,4,1408]{2,1,0:T(4,128)(2,1)S(1)}, u32[]{:S(2)}, u32[]{:S(2)}) async-start(bf16[64,4,1408]{2,1,0:T(4,128)(2,1)} %reshape.144), calls=%async_computation.1 | async-start | bytes 1441792 | tf_op jit(solution)/shard_map/all_to_all | solution.py:44
  67.3 22.7 %copy-start.4 = (bf16[704,32]{0,1:T(8,128)(2,1)S(1)}, bf16[704,32]{0,1:T(8,128)(2,1)}, u32[]{:S(2)}) copy-start(bf16[704,32]{0,1:T(8,128)(2,1)} %param.34) | copy-start | bytes 135172
  89.8 14.9 %copy-start.8 = (bf16[32,32]{1,0:T(8,128)(2,1)S(1)}, bf16[32,32]{1,0:T(8,128)(2,1)}, u32[]{:S(2)}) copy-start(bf16[32,32]{1,0:T(8,128)(2,1)} %param.30) | copy-start | bytes 6148
  90.0 24.4 %copy-start.26 = (s32[4]{0:T(128)S(1)}, s32[4]{0:T(128)}, u32[]{:S(2)}) copy-start(s32[4]{0:T(128)} %param.53) | copy-start | bytes 52
  90.0 29.3 %copy-start.24 = (f32[32]{0:T(128)S(1)}, f32[32]{0:T(128)}, u32[]{:S(2)}) copy-start(f32[32]{0:T(128)} %param.35) | copy-start | bytes 388
  90.0 29.3 %copy-start.10 = (bf16[32,256]{1,0:T(8,128)(2,1)S(1)}, bf16[32,256]{1,0:T(8,128)(2,1)}, u32[]{:S(2)}) copy-start(bf16[32,256]{1,0:T(8,128)(2,1)} %param.36) | copy-start | bytes 49156
  90.4 29.1 %copy-start.11 = (bf16[32,256]{1,0:T(8,128)(2,1)S(1)}, bf16[32,256]{1,0:T(8,128)(2,1)}, u32[]{:S(2)}) copy-start(bf16[32,256]{1,0:T(8,128)(2,1)} %param.37) | copy-start | bytes 49156
  91.2 18.2 %all-to-all-start.3 = ((bf16[8,2,512]{2,1,0:T(2,128)(2,1)}), bf16[8,2,512]{2,1,0:T(2,128)(2,1)S(1)}, u32[]{:S(2)}, u32[]{:S(2)}) async-start(bf16[8,2,512]{2,1,0:T(2,128)(2,1)} %reshape.174), calls=%async_computation.3 | async-start | bytes 32768 | tf_op jit(solution)/shard_map/all_to_all | solution.py:44
  109.5 10.3 %copy-start.16 = (bf16[32,32]{1,0:T(8,128)(2,1)S(1)}, bf16[32,32]{1,0:T(8,128)(2,1)}, u32[]{:S(2)}) copy-start(bf16[32,32]{1,0:T(8,128)(2,1)} %param.40) | copy-start | bytes 6148
  110.3 9.8 %copy-start.12 = (bf16[32,128]{1,0:T(8,128)(2,1)S(1)}, bf16[32,128]{1,0:T(8,128)(2,1)}, u32[]{:S(2)}) copy-start(bf16[32,128]{1,0:T(8,128)(2,1)} %param.38) | copy-start | bytes 24580
  110.3 8.8 %all-to-all-start.4 = ((bf16[8,2,512]{2,1,0:T(2,128)(2,1)}), bf16[8,2,512]{2,1,0:T(2,128)(2,1)S(1)}, u32[]{:S(2)}, u32[]{:S(2)}) async-start(bf16[8,2,512]{2,1,0:T(2,128)(2,1)} %reshape.176), calls=%async_computation.4 | async-start | bytes 32768 | tf_op jit(solution)/shard_map/all_to_all | solution.py:20
  119.2 1.1 copy-start.13
  120.5 5.9 %copy-start.14 = (f32[4,128,4]{1,2,0:T(4,128)S(1)}, f32[4,128,4]{1,2,0:T(4,128)}, u32[]{:S(2)}) copy-start(f32[4,128,4]{1,2,0:T(4,128)} %param.52) | copy-start | bytes 24580
  121.7 21.1 %all-to-all-start.5 = ((bf16[64,4,801]{2,1,0:T(4,128)(2,1)}), bf16[64,4,801]{2,1,0:T(4,128)(2,1)S(1)}, u32[]{:S(2)}, u32[]{:S(2)}) async-start(bf16[64,4,801]{2,1,0:T(4,128)(2,1)} %concatenate.26), calls=%async_computation.5 | async-start | bytes 917504 | tf_op jit(solution)/shard_map/all_to_all | solution.py:44
  126.4 0.7 copy-start.27
  126.4 1.0 copy-start.1
  126.6 0.9 copy-start.17
  126.6 0.9 copy-start.23
  126.7 1.0 copy-start.18
  126.7 1.0 copy-start.19
  126.7 1.0 copy-start.20
  126.7 1.0 copy-start.21
  126.7 1.0 copy-start.22
  127.0 16.8 %copy-start.2 = (bf16[4,128,128]{2,1,0:T(8,128)(2,1)S(1)}, bf16[4,128,128]{2,1,0:T(8,128)(2,1)}, u32[]{:S(2)}) copy-start(bf16[4,128,128]{2,1,0:T(8,128)(2,1)} %param.49) | copy-start | bytes 393220
  127.0 17.0 %copy-start.15 = (f32[4,128,4]{1,2,0:T(4,128)S(1)}, f32[4,128,4]{1,2,0:T(4,128)}, u32[]{:S(2)}) copy-start(f32[4,128,4]{1,2,0:T(4,128)} %param.51) | copy-start | bytes 24580
  144.1 19.2 %copy-start.9 = (bf16[256,32]{0,1:T(8,128)(2,1)S(1)}, bf16[256,32]{0,1:T(8,128)(2,1)}, u32[]{:S(2)}) copy-start(bf16[256,32]{0,1:T(8,128)(2,1)} %param.55) | copy-start | bytes 49156
  145.7 36.0 %copy-start.25 = (f32[32]{0:T(128)S(1)}, f32[32]{0:T(128)}, u32[]{:S(2)}) copy-start(f32[32]{0:T(128)} %param.56) | copy-start | bytes 388
  163.3 18.5 %copy-start.5 = (bf16[32,704]{1,0:T(8,128)(2,1)S(1)}, bf16[32,704]{1,0:T(8,128)(2,1)}, u32[]{:S(2)}) copy-start(bf16[32,704]{1,0:T(8,128)(2,1)} %param.58) | copy-start | bytes 135172
  163.5 18.6 %copy-start.6 = (bf16[32,704]{1,0:T(8,128)(2,1)S(1)}, bf16[32,704]{1,0:T(8,128)(2,1)}, u32[]{:S(2)}) copy-start(bf16[32,704]{1,0:T(8,128)(2,1)} %param.57) | copy-start | bytes 135172
  183.8 39.3 %all-to-all-start.9 = ((bf16[64,4,1408]{2,1,0:T(4,128)(2,1)}), bf16[64,4,1408]{2,1,0:T(4,128)(2,1)S(1)}, u32[]{:S(2)}, u32[]{:S(2)}) async-start(bf16[64,4,1408]{2,1,0:T(4,128)(2,1)} %reshape.155), calls=%async_computation.9 | async-start | bytes 1441792 | tf_op jit(solution)/shard_map/all_to_all | solution.py:44
  223.6 23.9 %copy-start.7 = (bf16[704,32]{0,1:T(8,128)(2,1)S(1)}, bf16[704,32]{0,1:T(8,128)(2,1)}, u32[]{:S(2)}) copy-start(bf16[704,32]{0,1:T(8,128)(2,1)} %param.59) | copy-start | bytes 135172
where the time goes:
time: 267 us; the launch traced here: 266 us
  blocking collectives  182 us (68%)
  starting transfers between devices  39.7 us (15%)
  waiting for transfers between devices  24.4 us (9%)
  local copies, waits for them, and re-layouts  10.9 us (4%)
  matrix products  4.68 us (2%)
  other arithmetic  3.69 us (1%)
    all_to_all x5, blocking collectives, copy_for_each(): lax.all_to_all(jnp.broadcast_to(shard[None], (size, *shard.shape)), axis,...  85.2 us
    psum x4, blocking collectives, by_axis(): shard = lax.psum(shard, axis)  69.6 us
    all_to_all x4, starting transfers between devices, sum_at_owner(): pieces = lax.all_to_all(cut_along(shard, dim, size), axis, 0, 0, tiled=True)  35.7 us
    all_to_all x2, blocking collectives, sum_at_owner(): pieces = lax.all_to_all(cut_along(shard, dim, size), axis, 0, 0, tiled=True)  27.1 us
    all_to_all x4, waiting for transfers between devices, sum_at_owner(): pieces = lax.all_to_all(cut_along(shard, dim, size), axis, 0, 0, tiled=True)  19.7 us
  transfers between devices with their start and end apart: 5, of which 3 were waited for; matrix products, arithmetic and copies ran while one was open for 1% of the time, Pallas kernels for 0%

commit v1 on v0

v1 whole, which is shorter than its diff:
```python
import jax
import jax.numpy as jnp
from jax import lax
from jax.experimental import pallas as pl
from jax.experimental.pallas import tpu as pltpu
from jax.sharding import Mesh
from jax.sharding import PartitionSpec as P

D = 2048
N = 8
ROWS = 32
OWN = 4
HID = 704
HIDP = 768
MIXW = 896
STEP_AT = 768
EPSILON = 1e-06
MESH = pl.DeviceIdType.MESH
F32 = jnp.float32
BF16 = jnp.bfloat16
HIGHEST = lax.Precision.HIGHEST


def at(z, y, t):
    return (z, y, t)


def plus(a, b):
    return lax.rem(a + b, N)


def dot_nt(a, b, precision=None):
    return lax.dot_general(
        a, b, (((1,), (1,)), ((), ())), precision=precision, preferred_element_type=F32
    )


def lanes(shape):
    return lax.broadcasted_iota(jnp.int32, shape, 1)


def silu(a):
    return a / (1.0 + jnp.exp(-a))


def softplus(a):
    return jnp.maximum(a, 0.0) + jnp.log1p(jnp.exp(-jnp.abs(a)))


class Ring:
    def __init__(self, buf, ahead, back, recv, me):
        self.buf, self.ahead, self.back, self.recv = buf, ahead, back, recv
        self.z, self.y, self.t = me

    def copy(self, slot, step, forward):
        to = plus(self.z, 1 if forward else N - 1)
        return pltpu.make_async_remote_copy(
            src_ref=self.buf.at[slot],
            dst_ref=self.buf.at[slot],
            send_sem=(self.ahead if forward else self.back).at[step],
            recv_sem=self.recv.at[slot],
            device_id=at(to, self.y, self.t),
            device_id_type=MESH,
        )

    def start(self):
        self.copy(self.z, 0, True).start()
        self.copy(self.z, 0, False).start()

    def arrived(self, slot):
        self.copy(slot, 0, True).wait_recv()

    def relay(self, k):
        slot = plus(self.z, N - k)
        self.arrived(slot)
        self.copy(slot, k, True).start()
        if k <= 2:
            slot = plus(self.z, k)
            self.arrived(slot)
            self.copy(slot, k, False).start()

    def finish(self):
        self.arrived(plus(self.z, N - 4))
        self.arrived(plus(self.z, 3))

    def drain(self):
        for k in range(4):
            self.copy(self.z, k, True).wait_send()
        for k in range(3):
            self.copy(self.z, k, False).wait_send()


class Group:
    def __init__(self, src, dst, send, recv, me, axis, scatter):
        self.src, self.dst, self.send, self.recv = src, dst, send, recv
        self.me, self.axis, self.scatter = me, axis, scatter
        self.own = me[axis]

    def copy(self, d):
        to = plus(self.own, d)
        target = list(self.me)
        target[self.axis] = to
        return pltpu.make_async_remote_copy(
            src_ref=self.src.at[to] if self.scatter else self.src.at[self.own],
            dst_ref=self.dst.at[self.own],
            send_sem=self.send.at[d],
            recv_sem=self.recv.at[self.own],
            device_id=tuple(target),
            device_id_type=MESH,
        )

    def start(self):
        def body(d, c):
            self.copy(d).start()
            return c

        lax.fori_loop(1, N, body, 0)

    def wait(self):
        def body(d, c):
            slot = plus(self.own, d)
            pltpu.make_async_remote_copy(
                src_ref=self.dst.at[slot],
                dst_ref=self.dst.at[slot],
                send_sem=self.send.at[d],
                recv_sem=self.recv.at[slot],
                device_id=self.me,
                device_id_type=MESH,
            ).wait_recv()
            return c

        lax.fori_loop(1, N, body, 0)

    def drain(self):
        def body(d, c):
            self.copy(d).wait_send()
            return c

        lax.fori_loop(1, N, body, 0)


def total(ref):
    acc = ref[0].astype(F32)
    for k in range(1, N):
        acc = acc + ref[k].astype(F32)
    return acc


def stacked(ref):
    return jnp.concatenate([ref[k].astype(F32) for k in range(N)], axis=0).astype(BF16)


def spread(blocks):
    halves = []
    for half in range(2):
        acc = blocks[4 * half]
        for k in range(1, 4):
            acc = acc + pltpu.roll(blocks[4 * half + k], 32 * k, 1)
        halves.append(acc)
    return jnp.concatenate(halves, axis=1)


def piece(values, k):
    half = values[:, 128 * (k // 4) : 128 * (k // 4) + 128]
    return half if k % 4 == 0 else pltpu.roll(half, 128 - 32 * (k % 4), 1)


def with_squares(part, values, at_lane):
    squares = jnp.sum(values * values, axis=1, keepdims=True)
    high = squares.astype(BF16).astype(F32)
    low = squares - high
    lane = lanes(part.shape)
    return jnp.where(lane == at_lane, high, jnp.where(lane == at_lane + 1, low, part))


def row_scale(summed, at_lane):
    squares = summed[:, at_lane : at_lane + 1] + summed[:, at_lane + 1 : at_lane + 2]
    return lax.rsqrt(squares / D + EPSILON)


def kernel(
    x_ref,
    gains_ref,
    gate1_ref,
    lift1_ref,
    drop1_ref,
    value_proj_ref,
    gate_proj_ref,
    key_proj_ref,
    query_proj_ref,
    step_proj_ref,
    value_taps_ref,
    key_taps_ref,
    query_taps_ref,
    value_past_ref,
    key_past_ref,
    query_past_ref,
    rate_ref,
    state_ref,
    keys_ref,
    values_ref,
    steps_ref,
    decay_ref,
    lengths_ref,
    head_gain_ref,
    out_proj_ref,
    gate2_ref,
    lift2_ref,
    drop2_ref,
    out_ref,
    x_own,
    x_all,
    gains_all,
    gate1_all,
    lift1_all,
    drop1_all,
    mix_all,
    proj_all,
    gate2_all,
    lift2_all,
    drop2_all,
    rs1_src,
    rs1_dst,
    h1_all,
    sum1_all,
    rsm_src,
    rsm_dst,
    hm_all,
    summ_all,
    rs2_src,
    rs2_dst,
    h2_all,
    two_src,
    two_dst,
    end_src,
    end_dst,
    ring_ahead,
    ring_back,
    ring_recv,
    group_send,
    group_recv,
    x_send,
    x_recv,
    end_send,
    end_recv,
    two_send,
    two_recv,
):
    z = lax.axis_index("z")
    y = lax.axis_index("y")
    t = lax.axis_index("t")
    me = (z, y, t)
    diagonal = z == t

    barrier = pltpu.get_barrier_semaphore()

    def hello(target):
        pl.semaphore_signal(barrier, inc=1, device_id=target, device_id_type=MESH)

    hello(at(plus(z, 1), y, t))
    hello(at(plus(z, N - 1), y, t))

    def greet(d, c):
        hello(at(z, plus(y, d), t))
        hello(at(z, y, plus(t, d)))
        hello(at(plus(z, d), y, z))
        hello(at(t, y, plus(t, d)))
        return c

    lax.fori_loop(1, N, greet, 0)

    @pl.when(jnp.logical_not(diagonal))
    def _():
        hello(at(z, y, z))
        hello(at(t, y, t))

    rings = {}
    for k, (name, buf) in enumerate(
        (
            ("gains", gains_all),
            ("gate1", gate1_all),
            ("lift1", lift1_all),
            ("drop1", drop1_all),
            ("mix", mix_all),
            ("proj", proj_all),
            ("gate2", gate2_all),
            ("lift2", lift2_all),
            ("drop2", drop2_all),
        )
    ):
        rings[name] = Ring(buf, ring_ahead.at[k], ring_back.at[k], ring_recv.at[k], me)

    groups = []

    def group(src, dst, axis, scatter):
        k = len(groups)
        groups.append(Group(src, dst, group_send.at[k], group_recv.at[k], me, axis, scatter))
        return groups[-1]

    eye = (
        lax.broadcasted_iota(jnp.int32, (ROWS, ROWS), 0) == lanes((ROWS, ROWS))
    ).astype(F32).astype(BF16)

    def pack_wide(buf, ref):
        buf[z, :, HID:HIDP] = jnp.zeros((ROWS, HIDP - HID), BF16)
        buf[z, :, 0:HID] = ref[...]

    def pack_drop(buf, ref):
        buf[z, :, HID:HIDP] = jnp.zeros((ROWS, HIDP - HID), BF16)
        buf[z, :, 0:HID] = dot_nt(eye, ref[...]).astype(BF16)

    x_own[...] = jnp.zeros((ROWS, 128), BF16)
    x_own[:, 0:32] = x_ref[...]
    gains_all[z] = gains_ref[...]
    pack_wide(gate1_all, gate1_ref)
    pack_wide(lift1_all, lift1_ref)
    pack_drop(drop1_all, drop1_ref)
    mix_all[z, :, 0:256] = value_proj_ref[...]
    mix_all[z, :, 256:512] = gate_proj_ref[...]
    mix_all[z, :, 512:640] = key_proj_ref[...]
    mix_all[z, :, 640:768] = query_proj_ref[...]
    mix_all[z, :, 768:896] = jnp.zeros((ROWS, 128), BF16)
    mix_all[z, :, 768:800] = step_proj_ref[...]
    proj_all[z] = dot_nt(eye, out_proj_ref[...]).astype(BF16)
    pack_wide(gate2_all, gate2_ref)
    pack_wide(lift2_all, lift2_ref)
    pack_drop(drop2_all, drop2_ref)

    pl.semaphore_wait(barrier, 32 - 2 * diagonal.astype(jnp.int32))

    def x_copy(d):
        return pltpu.make_async_remote_copy(
            src_ref=x_own,
            dst_ref=x_all.at[z],
            send_sem=x_send.at[d],
            recv_sem=x_recv.at[z],
            device_id=at(t, y, plus(t, d)),
            device_id_type=MESH,
        )

    def x_start(d, c):
        x_copy(d).start()
        return c

    lax.fori_loop(1, N, x_start, 0)

    @pl.when(jnp.logical_not(diagonal))
    def _():
        x_copy(0).start()

    @pl.when(diagonal)
    def _():
        x_all[z] = x_own[...]

    rings["gains"].start()
    rings["gate1"].start()
    rings["lift1"].start()
    rings["drop1"].start()

    for k in range(1, 4):
        rings["gains"].relay(k)
        rings["gate1"].relay(k)
        rings["lift1"].relay(k)

    rings["mix"].start()
    rings["proj"].start()
    rings["drop1"].relay(1)

    def x_wait(k):
        return pltpu.make_async_remote_copy(
            src_ref=x_all.at[k],
            dst_ref=x_all.at[k],
            send_sem=x_send.at[0],
            recv_sem=x_recv.at[k],
            device_id=me,
            device_id_type=MESH,
        )

    def x_arrived(d, c):
        x_wait(plus(z, d)).wait_recv()
        return c

    lax.fori_loop(1, N, x_arrived, 0)

    @pl.when(jnp.logical_not(diagonal))
    def _():
        x_wait(z).wait_recv()

    rings["gains"].finish()
    gains = spread([gains_all[k] for k in range(N)])
    section = spread([x_all[k].astype(F32) for k in range(N)])

    def unit_open(section, gain, gate_all, lift_all, rs_src, rs_dst):
        scaled = (section * gain).astype(BF16)
        gate = jnp.dot(scaled, gate_all[...].reshape(256, HIDP), preferred_element_type=F32)
        gate = with_squares(gate, section, HID)
        lift = jnp.dot(scaled, lift_all[...].reshape(256, HIDP), preferred_element_type=F32)
        for k in range(N):
            rs_src[k, :, 0:HIDP] = gate[OWN * k : OWN * k + OWN].astype(BF16)
            rs_src[k, :, HIDP:] = lift[OWN * k : OWN * k + OWN].astype(BF16)
        exchange = group(rs_src, rs_dst, 1, True)
        exchange.start()
        rs_dst[y] = rs_src[y]
        return exchange

    def unit_hidden(exchange, rs_dst, h_all):
        exchange.wait()
        summed = total(rs_dst)
        scale = row_scale(summed, HID)
        hidden = silu(summed[:, 0:HIDP] * scale) * (summed[:, HIDP:] * scale)
        h_all[y] = hidden.astype(BF16)
        gather = group(h_all, h_all, 1, False)
        gather.start()
        return gather

    def down(gather, h_all, weight_all, width):
        gather.wait()
        return dot_nt(stacked(h_all), weight_all[...].reshape(256, width))

    def share(part, sum_all):
        sum_all[t] = part.astype(BF16)
        shared = group(sum_all, sum_all, 2, False)
        shared.start()
        return shared

    rings["gate1"].finish()
    rings["lift1"].finish()
    exchange = unit_open(section, gains[0:1], gate1_all, lift1_all, rs1_src, rs1_dst)

    rings["drop1"].relay(2)
    rings["mix"].relay(1)
    rings["proj"].relay(1)
    gather = unit_hidden(exchange, rs1_dst, h1_all)

    rings["drop1"].relay(3)
    rings["gate2"].start()
    rings["lift2"].start()
    rings["mix"].relay(2)
    rings["proj"].relay(2)

    lane16 = lanes((16, 128))
    live = lane16 < lengths_ref[...] - 1
    masked = jnp.where(live, decay_ref[...], 0.0)
    later = (lax.broadcasted_iota(jnp.int32, (128, 128), 0) > lanes((128, 128))).astype(F32)
    tail = jnp.dot(masked, later, precision=HIGHEST, preferred_element_type=F32)
    decay_total = jnp.sum(masked, axis=1, keepdims=True)
    fading = jnp.where(live, jnp.exp(tail) * steps_ref[...], 0.0)

    def earlier(past_ref, taps_ref):
        rows = [
            jnp.sum(past_ref[s].astype(F32) * taps_ref[0:3, :], axis=0, keepdims=True)
            for s in range(OWN)
        ]
        return jnp.concatenate(rows, axis=0)

    value_earlier = earlier(value_past_ref, value_taps_ref)
    key_earlier = earlier(key_past_ref, key_taps_ref)
    query_earlier = earlier(query_past_ref, query_taps_ref)

    rings["drop1"].finish()
    shared = share(down(gather, h1_all, drop1_all, HIDP), sum1_all)
    rings["drop2"].start()
    rings["mix"].relay(3)
    rings["proj"].relay(3)
    shared.wait()
    section = (section + 0.5 * total(sum1_all)).astype(BF16).astype(F32)

    rings["mix"].finish()
    scaled = (section * gains[1:2]).astype(BF16)
    mix = jnp.dot(scaled, mix_all[...].reshape(256, MIXW), preferred_element_type=F32)
    mix = with_squares(mix, section, STEP_AT + 32)
    for k in range(N):
        rsm_src[k] = mix[OWN * k : OWN * k + OWN].astype(BF16)
    exchange = group(rsm_src, rsm_dst, 1, True)
    exchange.start()
    rsm_dst[y] = rsm_src[y]
    for name in ("gate2", "lift2", "drop2"):
        rings[name].relay(1)
    exchange.wait()
    summed = total(rsm_dst)
    summed = summed * row_scale(summed, STEP_AT + 32)
    new_value = silu(value_earlier + value_taps_ref[3:4, :] * summed[:, 0:256])
    gate_vals = silu(summed[:, 256:512])
    new_key = silu(key_earlier + key_taps_ref[3:4, :] * summed[:, 512:640])
    new_query = silu(query_earlier + query_taps_ref[3:4, :] * summed[:, 640:768])
    step_all = softplus(summed[:, 768:896])
    lane4 = lanes((OWN, 128))
    step = [
        jnp.sum(jnp.where(lane4 == OWN * t + j, step_all, 0.0), axis=1, keepdims=True)
        for j in range(4)
    ]
    fall = [-rate_ref[j] * step[j] for j in range(4)]
    self_score = jnp.sum(new_query * new_key, axis=1, keepdims=True)
    query8 = jnp.concatenate([new_query, jnp.zeros((OWN, 128), F32)], axis=0)
    query8_round = query8.astype(BF16)
    head_of = lanes((4, 256)) // 64
    own_head = head_of == lax.broadcasted_iota(jnp.int32, (4, 256), 0)
    rows = []
    for s in range(OWN):
        this_fall = jnp.concatenate([fall[j][s : s + 1] for j in range(4)], axis=0)
        this_step = jnp.concatenate([step[j][s : s + 1] for j in range(4)], axis=0)
        scores = dot_nt(query8_round, keys_ref[s])[s : s + 1]
        weights = (fading[4 * s : 4 * s + 4] * jnp.exp(this_fall) * scores).astype(BF16)
        weights8 = jnp.concatenate([weights.astype(F32), jnp.zeros((4, 128), F32)], axis=0)
        from_block = jnp.dot(
            weights8.astype(BF16), values_ref[s], preferred_element_type=F32
        )[0:4]
        from_state = dot_nt(query8, state_ref[s].reshape(256, 128), HIGHEST)[s : s + 1]
        from_state = jnp.exp(decay_total[4 * s : 4 * s + 4] + this_fall) * from_state
        from_token = (this_step * self_score[s : s + 1]) * new_value[s : s + 1]
        heads = from_state + from_block + from_token
        rows.append(jnp.sum(jnp.where(own_head, heads, 0.0), axis=0, keepdims=True))
    gated = jnp.concatenate(rows, axis=0) * gate_vals
    squares = gated * gated
    inverse = jnp.zeros((OWN, 256), F32)
    for j in range(4):
        mean = jnp.sum(jnp.where(head_of == j, squares, 0.0), axis=1, keepdims=True) / 64
        inverse = jnp.where(head_of == j, lax.rsqrt(mean + EPSILON), inverse)
    hm_all[y] = (gated * inverse * head_gain_ref[...]).astype(BF16)
    gather = group(hm_all, hm_all, 1, False)
    gather.start()
    for name in ("gate2", "lift2", "drop2"):
        rings[name].relay(2)
    rings["proj"].finish()
    shared = share(down(gather, hm_all, proj_all, 256), summ_all)
    for name in ("gate2", "lift2", "drop2"):
        rings[name].relay(3)
    shared.wait()
    section = (section + total(summ_all)).astype(BF16).astype(F32)

    rings["gate2"].finish()
    rings["lift2"].finish()
    exchange = unit_open(section, gains[2:3], gate2_all, lift2_all, rs2_src, rs2_dst)

    for k in range(N):
        two_src[k] = piece(section, k).astype(BF16)
    two_copy = pltpu.make_async_remote_copy(
        src_ref=two_src.at[t],
        dst_ref=two_dst,
        send_sem=two_send,
        recv_sem=two_recv,
        device_id=at(t, y, z),
        device_id_type=MESH,
    )

    @pl.when(jnp.logical_not(diagonal))
    def _():
        two_copy.start()

    @pl.when(diagonal)
    def _():
        two_dst[...] = two_src[t]

    gather = unit_hidden(exchange, rs2_dst, h2_all)
    rings["drop2"].finish()
    part = down(gather, h2_all, drop2_all, HIDP)
    for k in range(N):
        end_src[k] = piece(part, k).astype(BF16)

    def end_copy(d):
        to = plus(z, d)
        return pltpu.make_async_remote_copy(
            src_ref=end_src.at[to],
            dst_ref=end_dst.at[t],
            send_sem=end_send.at[d],
            recv_sem=end_recv.at[t],
            device_id=at(to, y, z),
            device_id_type=MESH,
        )

    def end_start(d, c):
        end_copy(d).start()
        return c

    lax.fori_loop(1, N, end_start, 0)

    @pl.when(jnp.logical_not(diagonal))
    def _():
        end_copy(0).start()

    @pl.when(diagonal)
    def _():
        end_dst[t] = end_src[z]

    def end_wait(k):
        return pltpu.make_async_remote_copy(
            src_ref=end_dst.at[k],
            dst_ref=end_dst.at[k],
            send_sem=end_send.at[0],
            recv_sem=end_recv.at[k],
            device_id=me,
            device_id_type=MESH,
        )

    for each in groups:
        each.drain()
    for each in rings.values():
        each.drain()

    def x_drain(d, c):
        x_copy(d).wait_send()
        return c

    lax.fori_loop(1, N, x_drain, 0)

    @pl.when(jnp.logical_not(diagonal))
    def _():
        x_copy(0).wait_send()
        two_copy.wait_send()
        two_copy.wait_recv()

    def end_arrived(d, c):
        end_wait(plus(t, d)).wait_recv()
        return c

    lax.fori_loop(1, N, end_arrived, 0)

    @pl.when(jnp.logical_not(diagonal))
    def _():
        end_wait(t).wait_recv()

    result = two_dst[...].astype(F32) + 0.5 * total(end_dst)
    out_ref[...] = result[:, 0:32].astype(BF16)

    def end_drain(d, c):
        end_copy(d).wait_send()
        return c

    lax.fori_loop(1, N, end_drain, 0)

    @pl.when(jnp.logical_not(diagonal))
    def _():
        end_copy(0).wait_send()


def on_device(
    hidden_in,
    gain_before,
    gate_before,
    lift_before,
    drop_before,
    mixer_gain,
    value_proj,
    gate_proj,
    key_proj,
    query_proj,
    step_proj,
    value_taps,
    key_taps,
    query_taps,
    value_past,
    key_past,
    query_past,
    decay_rate,
    block_state,
    block_keys,
    block_values,
    block_steps,
    block_decay,
    lengths,
    head_gain,
    out_proj,
    gain_after,
    gate_after,
    lift_after,
    drop_after,
):
    gains = jnp.pad(jnp.stack([gain_before, mixer_gain, gain_after]), ((0, 5), (0, 96)))
    by_head = lambda a: jnp.swapaxes(a, 1, 2).reshape(16, 128)
    args = (
        hidden_in,
        gains,
        gate_before,
        lift_before,
        drop_before,
        value_proj,
        gate_proj,
        key_proj,
        query_proj,
        step_proj,
        value_taps,
        key_taps,
        query_taps,
        value_past,
        key_past,
        query_past,
        decay_rate,
        block_state,
        block_keys,
        block_values,
        by_head(block_steps),
        by_head(block_decay),
        jnp.repeat(lengths, 4)[:, None],
        head_gain[None, :],
        out_proj,
        gate_after,
        lift_after,
        drop_after,
    )
    vmem = pl.BlockSpec(memory_space=pltpu.VMEM)
    smem = pl.BlockSpec(memory_space=pltpu.SMEM)
    wide = pltpu.VMEM((N, ROWS, HIDP), BF16)
    scratch = [
        pltpu.VMEM((ROWS, 128), BF16),
        pltpu.VMEM((N, ROWS, 128), BF16),
        pltpu.VMEM((N, 8, 128), F32),
        wide,
        wide,
        wide,
        pltpu.VMEM((N, ROWS, MIXW), BF16),
        pltpu.VMEM((N, ROWS, 256), BF16),
        wide,
        wide,
        wide,
        pltpu.VMEM((N, OWN, 2 * HIDP), BF16),
        pltpu.VMEM((N, OWN, 2 * HIDP), BF16),
        pltpu.VMEM((N, OWN, HIDP), BF16),
        pltpu.VMEM((N, ROWS, 256), BF16),
        pltpu.VMEM((N, OWN, MIXW), BF16),
        pltpu.VMEM((N, OWN, MIXW), BF16),
        pltpu.VMEM((N, OWN, 256), BF16),
        pltpu.VMEM((N, ROWS, 256), BF16),
        pltpu.VMEM((N, OWN, 2 * HIDP), BF16),
        pltpu.VMEM((N, OWN, 2 * HIDP), BF16),
        pltpu.VMEM((N, OWN, HIDP), BF16),
        pltpu.VMEM((N, ROWS, 128), BF16),
        pltpu.VMEM((ROWS, 128), BF16),
        pltpu.VMEM((N, ROWS, 128), BF16),
        pltpu.VMEM((N, ROWS, 128), BF16),
        pltpu.SemaphoreType.DMA((9, 4)),
        pltpu.SemaphoreType.DMA((9, 3)),
        pltpu.SemaphoreType.DMA((9, N)),
        pltpu.SemaphoreType.DMA((8, N)),
        pltpu.SemaphoreType.DMA((8, N)),
        pltpu.SemaphoreType.DMA((N,)),
        pltpu.SemaphoreType.DMA((N,)),
        pltpu.SemaphoreType.DMA((N,)),
        pltpu.SemaphoreType.DMA((N,)),
        pltpu.SemaphoreType.DMA,
        pltpu.SemaphoreType.DMA,
    ]
    return pl.pallas_call(
        kernel,
        out_shape=jax.ShapeDtypeStruct((ROWS, 32), BF16),
        in_specs=[smem if k == 16 else vmem for k in range(len(args))],
        out_specs=vmem,
        scratch_shapes=scratch,
        compiler_params=pltpu.CompilerParams(collective_id=0, has_side_effects=True),
    )(*args)


def solution(mesh):
    finer = Mesh(mesh.devices.reshape(N, N, N), ("z", "y", "t"))
    kv = ("z", "y")
    return jax.shard_map(
        on_device,
        mesh=finer,
        in_specs=(
            P("t", kv),
            P(kv),
            P(kv, "t"),
            P(kv, "t"),
            P("t", kv),
            P(kv),
            P(kv, "t"),
            P(kv, "t"),
            P(kv, "t"),
            P(kv, "t"),
            P(kv, None),
            P(None, "t"),
            P(None, "t"),
            P(None, "t"),
            P(kv, None, "t"),
            P(kv, None, "t"),
            P(kv, None, "t"),
            P("t"),
            P(kv, "t", None, None),
            P(kv, None, "t"),
            P(kv, None, "t"),
            P(kv, None, "t"),
            P(kv, None, "t"),
            P(kv),
            P("t"),
            P("t", kv),
            P(kv),
            P(kv, "t"),
            P(kv, "t"),
            P("t", kv),
        ),
        out_specs=P("t", kv),
        check_vma=False,
    )
```

time: 267 us -> 93.9 us (0.35)
  blocking collectives: 182 us -> 0 us
  Pallas kernels: 0 us -> 84.8 us
  starting transfers between devices: 39.7 us -> 0 us
  waiting for transfers between devices: 24.4 us -> 0 us
  matrix products: 4.68 us -> 0 us
  local copies, waits for them, and re-layouts: 10.9 us -> 7.51 us
  other arithmetic: 3.69 us -> 0.59 us
    all_to_all x7 -> x0, blocking collectives: 112 us -> none  [the longest x5 85.2 us: copy_for_each(): lax.all_to_all(jnp.broadcast_to(shard[None], (size, *shard.shape)), axis,...]
    pallas_call x0 -> x1, Pallas kernels: none -> 84.8 us  [on_device(): pl.pallas_call(kernel, out_shape=jax.ShapeDtypeStruct((ROWS, 32), BF16),...]
    psum x4 -> x0, blocking collectives: 69.6 us -> none  [by_axis(): shard = lax.psum(shard, axis)]
    all_to_all x5 -> x0, starting transfers between devices: 39.7 us -> none  [the longest x4 35.7 us: sum_at_owner(): pieces = lax.all_to_all(cut_along(shard, dim, size), axis, 0, 0, tiled=True)]
    all_to_all x5 -> x0, waiting for transfers between devices: 24.4 us -> none  [the longest x4 19.7 us: sum_at_owner(): pieces = lax.all_to_all(cut_along(shard, dim, size), axis, 0, 0, tiled=True)]
    dot_general x15 -> x0, matrix products: 4.68 us -> none  [the longest x2 1.41 us: half_mlp(): lift_part = jnp.dot(scaled, lift_weight, preferred_element_type=jnp.float32)]
    unnamed x70 -> x27, local copies, waits for them, and re-layouts: 3.11 us -> 6.78 us
    reshape x14 -> x0, local copies, waits for them, and re-layouts: 3.08 us -> none  [the longest x8 2.52 us: cut_along(): shard.reshape(*shape[:dim], size, shape[dim] // size, *shape[dim + 1:])]
  transfers between devices with their start and end apart: 5 -> 0, of which waited for: 3 -> 0; matrix products, arithmetic and copies ran while one was open for 1% -> 0% of each run, Pallas kernels for 0% -> 0%
where the time goes in v1:
time: 93.9 us; the launch traced here: 93 us
  Pallas kernels  84.8 us (90%)
  local copies, waits for them, and re-layouts  7.51 us (8%)
    pallas_call x1, Pallas kernels, on_device(): pl.pallas_call(kernel, out_shape=jax.ShapeDtypeStruct((ROWS, 32), BF16),...  84.8 us
    unnamed x27, local copies, waits for them, and re-layouts  6.78 us

profile of v1, /device:TPU:1, one launch (start us, length us, event | category | flops | bytes accessed | tf_op | source)
XLA Modules:
  0.0 93.0 jit_solution(7502417790386424952)
XLA Ops:
  0.0 0.0 copy-start.6
  0.0 0.7 copy-done.6
  0.7 0.0 copy-start.7
  0.7 0.0 copy-start.8
  0.7 0.0 copy-start.9
  0.7 0.1 broadcast_in_dim.6
  0.7 0.6 copy-done.7
  1.3 0.0 copy-done.8
  1.3 0.0 copy-done.9
  1.3 0.0 copy-start.4
  1.3 0.0 copy-start.5
  1.3 0.6 select_maximum_fusion.gains_ref
  1.9 0.1 copy-done.4
  2.0 0.0 copy-start.3
  2.0 0.6 copy.33.key_past_ref
  2.6 0.0 copy-done.5
  2.6 0.0 copy-start.2
  2.6 0.6 copy.34.query_past_ref
  3.2 0.7 broadcast_in_dim_reshape.4.lengths_ref
  3.9 0.0 copy-done.3
  3.9 0.0 copy-start
  3.9 0.6 copy.32.value_past_ref
  4.5 0.0 copy-done.2
  4.5 0.7 copy.36.out_proj_ref
  5.2 0.0 copy-done
  5.2 0.0 copy-start.1
  5.2 0.8 copy.31.drop1_ref
  6.0 0.0 copy-done.1
  6.0 0.8 copy.37.drop2_ref
  6.8 84.8 %shard_map.280 = bf16[32,32]{1,0:T(8,128)(2,1)} custom-call(bf16[32,32]{1,0:T(8,128)(2,1)} %x_ref.1, f32[8,128]{1,0:T(8,128)} %select_maximum_fusion.gains_ref, bf16[32,704]{1,0:T(8,128)(2,1)} %gate1_ref.1, bf16[32,704]{1,0:T(8,128)(2,1)} %lift1_ref.1, bf16[704,32]{1,0:T(8,128)(2,1)} %copy.31.drop1_ref, bf16[32,256]{1,0:T(8,128)(2,1)} %value_proj_ref.1, ...), custom_call_target="tpu_custom_call" | custom-call | tf_op jit(solution)/shard_map/pallas_call | solution.py:742
  91.7 1.3 %copy.39 = bf16[32,32]{1,0:T(8,128)(2,1)} copy(bf16[32,32]{1,0:T(8,128)(2,1)} %shard_map.280) | data formatting | bytes 4096
Async XLA Ops:
  0.0 0.7 copy-start.6
  0.7 0.7 copy-start.7
  0.7 0.7 copy-start.8
  0.7 0.7 copy-start.9
  1.3 0.7 copy-start.4
  1.3 1.3 %copy-start.5 = (bf16[4,3,128]{2,0,1:T(4,128)(2,1)S(1)}, bf16[4,3,128]{2,0,1:T(4,128)(2,1)}, u32[]{:S(2)}) copy-start(bf16[4,3,128]{2,0,1:T(4,128)(2,1)} %param.46) | copy-start | bytes 9220
  2.0 1.9 %copy-start.3 = (bf16[4,3,256]{2,0,1:T(4,128)(2,1)S(1)}, bf16[4,3,256]{2,0,1:T(4,128)(2,1)}, u32[]{:S(2)}) copy-start(bf16[4,3,256]{2,0,1:T(4,128)(2,1)} %param.44) | copy-start | bytes 18436
  2.6 1.9 %copy-start.2 = (bf16[256,32]{0,1:T(8,128)(2,1)S(1)}, bf16[256,32]{0,1:T(8,128)(2,1)}, u32[]{:S(2)}) copy-start(bf16[256,32]{0,1:T(8,128)(2,1)} %param.55) | copy-start | bytes 49156
  3.9 1.3 %copy-start = (bf16[704,32]{0,1:T(8,128)(2,1)S(1)}, bf16[704,32]{0,1:T(8,128)(2,1)}, u32[]{:S(2)}) copy-start(bf16[704,32]{0,1:T(8,128)(2,1)} %param.34) | copy-start | bytes 135172
  5.2 0.8 copy-start.1
